TPU v7x, 32 devices: a whole 2x2x4 slice. The times are simulated.
32 devices in a mesh: ra: 8 (over z, y), cb: 4 (over x, core).
Axes of the slice: x: 2, y: 2, z: 4, core: 2. Of those that a mesh axis runs over, the one named last changes fastest.
Arguments:
- stream: bfloat16 [64, 1024], P(None, 'ra'), may hold values from -24 to 24, as said below
- gain_first: float32 [1024], P('ra'), may hold values from 0.5 to 1.5
- up_first: float32 [1024, 4096], P('ra', 'cb'), may hold values from -0.1875 to 0.1875
- down_first: float32 [4096, 1024], P('cb', 'ra'), may hold values from -0.09375 to 0.09375
- gain_second: float32 [1024], P('ra'), may hold values from 0.5 to 1.5
- up_second: float32 [1024, 4096], P('ra', 'cb'), may hold values from -0.1875 to 0.1875
- down_second: float32 [4096, 1024], P('cb', 'ra'), may hold values from -0.09375 to 0.09375
Outputs:
- read: bfloat16 [64, 1024], P(None, 'ra')
Inputs may be any that keep to these rules, and one draw needn't show every extreme that they name: stream is of order one, and in each token one aligned block of 128 features is four times larger than the rest.
All inputs are finite; a program needn't handle non-finite values.
Results may differ from a plain program's by a relative error of at most 0.025.
Values may be sent and summed in bfloat16 or wider, within the bound.
A program may use at most 64 MiB of HBM per device.

v0:
```python
import jax
import jax.numpy as jnp
from jax import lax
from jax.sharding import PartitionSpec as P

D = 1024
EPS = 1e-06
RESIDUAL = 0.25


def sublayer(stream, norm_gain, w_up, w_down):
    floated = stream.astype(jnp.float32)
    own_squares = jnp.sum(floated * floated, axis=1, keepdims=True)
    squares = lax.psum(own_squares, "ra")
    factor = lax.rsqrt(squares / D + EPS)
    normed = (floated * factor * norm_gain.astype(jnp.float32)[None, :]).astype(jnp.bfloat16)
    up_bf = w_up.astype(jnp.bfloat16)
    down_bf = w_down.astype(jnp.bfloat16)
    partial_value = jnp.dot(normed, up_bf, preferred_element_type=jnp.float32)
    preact = lax.psum(partial_value, "ra")
    activated = jnp.square(jax.nn.relu(preact)).astype(jnp.bfloat16)
    down_part = jnp.dot(activated, down_bf, preferred_element_type=jnp.float32)
    branch = lax.psum(down_part.astype(jnp.bfloat16), "cb").astype(jnp.float32)
    return (RESIDUAL * floated + branch).astype(jnp.bfloat16)


def local(stream, gain_first, up_first, down_first, gain_second, up_second, down_second):
    middle = sublayer(stream, gain_first, up_first, down_first)
    return sublayer(middle, gain_second, up_second, down_second)


def solution(mesh):
    return jax.shard_map(
        local,
        mesh=mesh,
        in_specs=(
            P(None, "ra"),
            P("ra"),
            P("ra", "cb"),
            P("cb", "ra"),
            P("ra"),
            P("ra", "cb"),
            P("cb", "ra"),
        ),
        out_specs=P(None, "ra"),
        check_vma=False,
    )
```

profile of v0, /device:TPU:0, one launch (start us, length us, event | category | flops | bytes accessed | tf_op | source)
XLA Modules:
  0.0 221.5 jit_solution(7013383935762173612)
XLA Ops:
  6.5 0.0 copy-start.3
  6.5 0.0 all-reduce.3.cloned.1.call-start
  6.5 0.9 fusion.10
  7.4 23.2 %psum.42 = f32[64,1]{0,1:T(1,128)S(1)} all-reduce(f32[64,1]{0,1:T(1,128)S(1)} %bitcast.7), channel_id=1, replica_groups=mesh['ra'=8,'cb'=4] {'ra'}, use_global_device_ids=true, to_apply=%region_1.0 | all-reduce | flops 64 | bytes 512 | tf_op jit(solution)/shard_map/psum | solution.py:14
  30.6 0.0 copy-start.4
  30.6 0.0 copy-done.3
  30.6 0.6 copy-done.4
  31.2 0.0 copy-start.1
  31.2 2.0 fusion.4
  33.3 0.0 copy-start
  33.3 0.0 all-reduce.3.cloned.1.call-update
  33.3 0.0 all-reduce.5.cloned.1.call-start
  33.4 68.4 %all-reduce.3.cloned.1.call-done = f32[64,1024]{1,0:T(8,128)} async-done(((f32[64,1024]{1,0:T(8,128)}), f32[64,1024]{1,0:T(8,128)}) %all-reduce.3.cloned.1.call-update) | async-done | bytes 262160 | tf_op jit(solution)/shard_map/psum | solution.py:20
  101.7 0.0 copy-done.1
  101.7 1.1 convolution_convert_fusion.1
  102.8 10.1 %psum.44 = bf16[64,128]{1,0:T(8,128)(2,1)S(1)} all-reduce(bf16[64,128]{1,0:T(8,128)(2,1)S(1)} %convolution_convert_fusion.1), channel_id=1, replica_groups=mesh['ra'=8,'cb'=4] {'cb'}, use_global_device_ids=true, to_apply=%region_3.4 | all-reduce | flops 8192 | bytes 32768 | tf_op jit(solution)/shard_map/psum | solution.py:23
  113.0 0.1 fusion.15
  113.1 19.6 %psum.45 = f32[64,1]{0,1:T(1,128)S(1)} all-reduce(f32[64,1]{0,1:T(1,128)S(1)} %bitcast.6), channel_id=1, replica_groups=mesh['ra'=8,'cb'=4] {'ra'}, use_global_device_ids=true, to_apply=%region_5.6 | all-reduce | flops 64 | bytes 512 | tf_op jit(solution)/shard_map/psum | solution.py:14
  132.7 0.0 copy-start.5
  132.7 0.0 copy-done
  132.7 0.6 copy-done.5
  133.3 0.0 copy-start.2
  133.3 0.9 fusion.1
  134.3 0.0 all-reduce.5.cloned.1.call-update
  134.3 68.5 %all-reduce.5.cloned.1.call-done = f32[64,1024]{1,0:T(8,128)} async-done(((f32[64,1024]{1,0:T(8,128)}), f32[64,1024]{1,0:T(8,128)}) %all-reduce.5.cloned.1.call-update) | async-done | bytes 262160 | tf_op jit(solution)/shard_map/psum | solution.py:20
  202.8 0.0 copy-done.2
  202.8 1.1 convolution_convert_fusion
  203.9 10.1 %psum.47 = bf16[64,128]{1,0:T(8,128)(2,1)S(1)} all-reduce(bf16[64,128]{1,0:T(8,128)(2,1)S(1)} %convolution_convert_fusion), channel_id=1, replica_groups=mesh['ra'=8,'cb'=4] {'cb'}, use_global_device_ids=true, to_apply=%region_7.8 | all-reduce | flops 8192 | bytes 32768 | tf_op jit(solution)/shard_map/psum | solution.py:23
  214.1 0.6 fusion.14
  (2 shorter events, 0.0 us)
Async XLA Ops:
  6.5 24.1 %copy-start.3 = (bf16[64,128]{1,0:T(8,128)(2,1)S(1)}, bf16[64,128]{1,0:T(8,128)(2,1)}, u32[]{:S(2)}) copy-start(bf16[64,128]{1,0:T(8,128)(2,1)} %param.7) | copy-start | bytes 49156
  6.5 95.2 %all-reduce.3.cloned.1.call-start = ((), (), s32[]{:S(2)}) async-start(), calls=%async_computation | async-start | bytes 524288 | tf_op jit(solution)/shard_map/psum | solution.py:20
  30.6 0.7 copy-start.4
  31.2 70.5 %copy-start.1 = (f32[1024,128]{1,0:T(8,128)S(1)}, f32[1024,128]{1,0:T(8,128)}, u32[]{:S(2)}) copy-start(f32[1024,128]{1,0:T(8,128)} %param.10) | copy-start | bytes 1572868
  33.3 99.4 %copy-start = (f32[128,1024]{1,0:T(8,128)S(1)}, f32[128,1024]{1,0:T(8,128)}, u32[]{:S(2)}) copy-start(f32[128,1024]{1,0:T(8,128)} %param.12) | copy-start | bytes 1572868
  33.3 169.5 %all-reduce.5.cloned.1.call-start = ((), (), s32[]{:S(2)}) async-start(), calls=%async_computation.1 | async-start | bytes 524288 | tf_op jit(solution)/shard_map/psum | solution.py:20
  132.7 0.7 copy-start.5
  133.3 69.5 %copy-start.2 = (f32[1024,128]{1,0:T(8,128)S(1)}, f32[1024,128]{1,0:T(8,128)}, u32[]{:S(2)}) copy-start(f32[1024,128]{1,0:T(8,128)} %param.13) | copy-start | bytes 1572868
Sparse Core Ops, SparseCore 0:
  33.4 68.2 all-reduce.2
  134.4 68.3 all-reduce.4
where the time goes:
time: 222 us
  waiting for transfers between devices  137 us (62%)
  blocking collectives  63 us (28%)
  between operations  13.4 us (6%)
  matrix products  5.2 us (2%)
    psum x2, waiting for transfers between devices, sublayer(): preact = lax.psum(partial_value, 'ra')  137 us
    psum x2, blocking collectives, sublayer(): squares = lax.psum(own_squares, 'ra')  42.8 us
    psum x2, blocking collectives, sublayer(): branch = lax.psum(down_part.astype(jnp.bfloat16), 'cb').astype(jnp.float32)  20.2 us
  transfers between devices with their start and end apart: 2, of which 2 were waited for; matrix products, arithmetic and copies ran while one was open for 0% of the time, Pallas kernels for 0%

commit v1 on v0

--- a/solution.py
+++ b/solution.py
@@ -20,7 +20,9 @@
     preact = lax.psum(partial_value, "ra")
     activated = jnp.square(jax.nn.relu(preact)).astype(jnp.bfloat16)
     down_part = jnp.dot(activated, down_bf, preferred_element_type=jnp.float32)
-    branch = lax.psum(down_part.astype(jnp.bfloat16), "cb").astype(jnp.float32)
+    branch = jnp.sum(lax.all_gather(down_part.astype(jnp.bfloat16), "cb"), axis=0).astype(
+        jnp.float32
+    )
     return (RESIDUAL * floated + branch).astype(jnp.bfloat16)
 
 

time: 222 us -> 212 us (0.955)
  blocking collectives: 63 us -> 53.2 us
    psum x2 -> x0, blocking collectives: 20.2 us -> none  [sublayer(): branch = lax.psum(down_part.astype(jnp.bfloat16), 'cb').astype(jnp.float32)]
    all_gather x0 -> x2, blocking collectives: none -> 10.5 us  [sublayer(): lax.all_gather(down_part.astype(jnp.bfloat16), 'cb')]
where the time goes in v1:
time: 212 us
  waiting for transfers between devices  137 us (65%)
  blocking collectives  53.2 us (25%)
  between operations  13.5 us (6%)
  matrix products  5.2 us (2%)
    psum x2, waiting for transfers between devices, sublayer(): preact = lax.psum(partial_value, 'ra')  137 us
    psum x2, blocking collectives, sublayer(): squares = lax.psum(own_squares, 'ra')  42.8 us
    all_gather x2, blocking collectives, sublayer(): lax.all_gather(down_part.astype(jnp.bfloat16), 'cb')  10.5 us
  transfers between devices with their start and end apart: 2, of which 2 were waited for; matrix products, arithmetic and copies ran while one was open for 0% of the time, Pallas kernels for 0%

profile of v1, /device:TPU:0, one launch (start us, length us, event | category | flops | bytes accessed | tf_op | source)
XLA Modules:
  0.0 211.6 jit_solution(10804062702338490355)
XLA Ops:
  6.5 0.0 copy-start.3
  6.5 0.0 all-reduce.3.cloned.1.call-start
  6.5 0.9 fusion.10
  7.4 23.2 %psum.28 = f32[64,1]{0,1:T(1,128)S(1)} all-reduce(f32[64,1]{0,1:T(1,128)S(1)} %bitcast.11), channel_id=1, replica_groups=mesh['ra'=8,'cb'=4] {'ra'}, use_global_device_ids=true, to_apply=%region_1.0 | all-reduce | flops 64 | bytes 512 | tf_op jit(solution)/shard_map/psum | solution.py:14
  30.6 0.0 copy-start.4
  30.6 0.0 copy-done.3
  30.6 0.6 copy-done.4
  31.2 0.0 copy-start.1
  31.2 2.0 fusion.4
  33.3 0.0 all-reduce.3.cloned.1.call-update
  33.3 0.0 copy-start
  33.3 0.0 all-reduce.5.cloned.1.call-start
  33.4 68.3 %all-reduce.3.cloned.1.call-done = f32[64,1024]{1,0:T(8,128)} async-done(((f32[64,1024]{1,0:T(8,128)}), f32[64,1024]{1,0:T(8,128)}) %all-reduce.3.cloned.1.call-update) | async-done | bytes 262160 | tf_op jit(solution)/shard_map/psum | solution.py:20
  101.7 0.0 copy-done.1
  101.7 1.1 convolution_convert_fusion.1
  102.8 5.2 %all-gather = bf16[256,128]{1,0:T(8,128)(2,1)S(1)} all-gather(bf16[64,128]{1,0:T(8,128)(2,1)S(1)} %convolution_convert_fusion.1), channel_id=2, replica_groups=mesh['ra'=8,'cb'=4] {'cb'}, dimensions={0}, use_global_device_ids=true | all-gather | bytes 81920 | tf_op jit(solution)/shard_map/all_gather | solution.py:23
  108.1 0.1 fusion.15
  108.2 19.6 %psum.30 = f32[64,1]{0,1:T(1,128)S(1)} all-reduce(f32[64,1]{0,1:T(1,128)S(1)} %bitcast.10), channel_id=1, replica_groups=mesh['ra'=8,'cb'=4] {'ra'}, use_global_device_ids=true, to_apply=%region_5.6 | all-reduce | flops 64 | bytes 512 | tf_op jit(solution)/shard_map/psum | solution.py:14
  127.8 0.0 copy-start.5
  127.8 0.0 copy-done
  127.8 0.6 copy-done.5
  128.5 0.0 copy-start.2
  128.5 0.9 fusion.1
  129.4 0.0 all-reduce.5.cloned.1.call-update
  129.4 68.4 %all-reduce.5.cloned.1.call-done = f32[64,1024]{1,0:T(8,128)} async-done(((f32[64,1024]{1,0:T(8,128)}), f32[64,1024]{1,0:T(8,128)}) %all-reduce.5.cloned.1.call-update) | async-done | bytes 262160 | tf_op jit(solution)/shard_map/psum | solution.py:20
  197.8 0.0 copy-done.2
  197.8 1.1 convolution_convert_fusion
  198.9 5.2 %all-gather.1 = bf16[256,128]{1,0:T(8,128)(2,1)S(1)} all-gather(bf16[64,128]{1,0:T(8,128)(2,1)S(1)} %convolution_convert_fusion), channel_id=3, replica_groups=mesh['ra'=8,'cb'=4] {'cb'}, dimensions={0}, use_global_device_ids=true | all-gather | bytes 81920 | tf_op jit(solution)/shard_map/all_gather | solution.py:23
  204.2 0.6 fusion.14
  (4 shorter events, 0.0 us)
Async XLA Ops:
  6.5 24.1 %copy-start.3 = (bf16[64,128]{1,0:T(8,128)(2,1)S(1)}, bf16[64,128]{1,0:T(8,128)(2,1)}, u32[]{:S(2)}) copy-start(bf16[64,128]{1,0:T(8,128)(2,1)} %param.7) | copy-start | bytes 49156
  6.5 95.2 %all-reduce.3.cloned.1.call-start = ((), (), s32[]{:S(2)}) async-start(), calls=%async_computation | async-start | bytes 524288 | tf_op jit(solution)/shard_map/psum | solution.py:20
  30.6 0.7 copy-start.4
  31.2 70.5 %copy-start.1 = (f32[1024,128]{1,0:T(8,128)S(1)}, f32[1024,128]{1,0:T(8,128)}, u32[]{:S(2)}) copy-start(f32[1024,128]{1,0:T(8,128)} %param.10) | copy-start | bytes 1572868
  33.3 94.5 %copy-start = (f32[128,1024]{1,0:T(8,128)S(1)}, f32[128,1024]{1,0:T(8,128)}, u32[]{:S(2)}) copy-start(f32[128,1024]{1,0:T(8,128)} %param.12) | copy-start | bytes 1572868
  33.3 164.5 %all-reduce.5.cloned.1.call-start = ((), (), s32[]{:S(2)}) async-start(), calls=%async_computation.1 | async-start | bytes 524288 | tf_op jit(solution)/shard_map/psum | solution.py:20
  127.8 0.7 copy-start.5
  128.5 69.3 %copy-start.2 = (f32[1024,128]{1,0:T(8,128)S(1)}, f32[1024,128]{1,0:T(8,128)}, u32[]{:S(2)}) copy-start(f32[1024,128]{1,0:T(8,128)} %param.13) | copy-start | bytes 1572868
Sparse Core Ops, SparseCore 0:
  33.4 68.2 all-reduce.2
  129.5 68.2 all-reduce.4
